TPU v7x, 32 devices: a whole 2x2x4 slice. The times are simulated.
32 devices in a mesh: ep: 4 (over y, x), tp: 8 (over z, core).
Axes of the slice: x: 2, y: 2, z: 4, core: 2. Of those that a mesh axis runs over, the one named last changes fastest.
Arguments:
- queries: bfloat16 [3072, 2048], P('ep', 'tp'), may hold values from -6 to 6
- keys: bfloat16 [3072, 512], P('ep'), may hold values from -6 to 6
- values: bfloat16 [3072, 512], P('ep'), may hold values from -6 to 6
- query_gain: float32 [128], replicated, may hold values from 1 to 4.5
- key_gain: float32 [128], replicated, may hold values from 1 to 4.5
- out_weight: bfloat16 [2048, 2048], P('tp'), may hold values from -0.75 to 0.75
- tokens_b: bfloat16 [1536, 2048], P('ep'), may hold values from -6 to 6
- norm_gain: float32 [2048], replicated, may hold values from 0.1 to 1.9
- routes: int32 [1536, 2], P('ep'), may hold values from 0 to 15, all different within a row; in each aligned block of 48 rows (0 to 47, 48 to 95, ...) at most 8 rows name the same one
- route_weight: float32 [1536, 2], P('ep'), may hold values from 0.2 to 1
- gate_weight: bfloat16 [16, 2048, 4096], P('ep', None, 'tp'), may hold values from -0.125 to 0.125
- up_weight: bfloat16 [16, 2048, 4096], P('ep', None, 'tp'), may hold values from -0.125 to 0.125
- down_weight: bfloat16 [16, 4096, 2048], P('ep', 'tp'), may hold values from -0.09375 to 0.09375
Outputs:
- mixed_out: bfloat16 [3072, 2048], P(('ep', 'tp'))
- expert_out: bfloat16 [1536, 2048], P(('ep', 'tp'))
Inputs may be any that keep to these rules, and one draw needn't show every extreme that they name: `routes`: A row names 2 different experts. In each aligned block of 48 rows no expert is named more than 8 times, a bound that some block reaches.
All inputs are finite; a program needn't handle non-finite values.
Results may differ from a plain program's by a relative error of at most 0.019.
Values may be sent and summed in bfloat16 or wider, within the bound.
A program may use at most 128 MiB of HBM per device.

v0:
```python
import jax
import jax.numpy as jnp
from jax import lax
from jax.sharding import PartitionSpec as P

D = 2048
HD = 128
HQ = 16
KVH = 4
EXPERTS = 16
TOPK = 2
GRID_W = 64
CAP = 8


EPS = 1e-06
THETA = 10000.0


def rotate(field, positions):
    n_freq = HD // 4
    row_pos = (positions // GRID_W).astype(jnp.float32)
    col_pos = (positions % GRID_W).astype(jnp.float32)
    inverse = THETA ** (-jnp.arange(n_freq, dtype=jnp.float32) / n_freq)
    angles = jnp.stack([row_pos[:, None] * inverse, col_pos[:, None] * inverse], axis=1)
    cosine = jnp.cos(angles)[:, None]
    sine = jnp.sin(angles)[:, None]
    length, n_heads = (field.shape[0], field.shape[1])
    halves = field.reshape(length, n_heads, 2, 2, n_freq)
    leading = halves[..., 0, :]
    second = halves[..., 1, :]
    turned = jnp.stack(
        [leading * cosine - second * sine, second * cosine + leading * sine], axis=-2
    )
    return turned.reshape(length, n_heads, HD)


def prepare(source, gain_vec, positions, n_heads):
    length = source.shape[0]
    field = source.astype(jnp.float32).reshape(length, n_heads, HD)
    field = field * lax.rsqrt(jnp.mean(field * field, axis=-1, keepdims=True) + EPS) * gain_vec
    return rotate(field, positions).astype(jnp.bfloat16)


def token_mixer(queries, keys, values, query_gain, key_gain, out_weight):
    n_rows = queries.shape[0]
    q_heads = queries.shape[1] // HD
    positions = lax.axis_index("ep") * n_rows + jnp.arange(n_rows, dtype=jnp.int32)
    query_n = prepare(queries, query_gain, positions, q_heads).reshape(n_rows * q_heads, HD)
    kv_index = lax.axis_index("tp") * q_heads // (HQ // KVH)
    own_keys = prepare(
        lax.dynamic_slice_in_dim(keys, kv_index * HD, HD, 1), key_gain, positions, 1
    ).reshape(n_rows, HD)
    own_values = lax.dynamic_slice_in_dim(values, kv_index * HD, HD, 1)
    score_scale = HD ** (-0.5)
    start_state = (
        jnp.full((n_rows * q_heads,), -1e30, jnp.float32),
        jnp.zeros((n_rows * q_heads,), jnp.float32),
        jnp.zeros((n_rows * q_heads, HD), jnp.float32),
    )
    key_piece = lax.all_gather(own_keys, "ep", axis=0, tiled=True)
    value_piece = lax.all_gather(own_values, "ep", axis=0, tiled=True)
    steps_n = key_piece.shape[0] // n_rows

    def one_block(index_b, state):
        running_max, totals, numerator = state
        key_blk = lax.dynamic_slice_in_dim(key_piece, index_b * n_rows, n_rows, 0)
        value_blk = lax.dynamic_slice_in_dim(value_piece, index_b * n_rows, n_rows, 0)
        scores = (
            jnp.einsum("qd,sd->qs", query_n, key_blk, preferred_element_type=jnp.float32)
            * score_scale
        )
        new_max = jnp.maximum(running_max, jnp.max(scores, axis=1))
        shrink = jnp.exp(running_max - new_max)
        weights = jnp.exp(scores - new_max[:, None])
        totals = totals * shrink + jnp.sum(weights, axis=1)
        numerator = numerator * shrink[:, None] + jnp.dot(
            weights.astype(jnp.bfloat16), value_blk, preferred_element_type=jnp.float32
        )
        return (new_max, totals, numerator)

    running_max, totals, numerator = lax.fori_loop(0, steps_n, one_block, start_state)
    attended = (numerator / totals[:, None]).astype(jnp.bfloat16).reshape(n_rows, q_heads * HD)
    return lax.psum_scatter(
        jnp.dot(attended, out_weight, preferred_element_type=jnp.float32).astype(jnp.bfloat16),
        "tp",
        scatter_dimension=0,
        tiled=True,
    )


def expert_half(tokens_b, norm_gain, routes, route_weight, gate_weight, up_weight, down_weight):
    n_tp = lax.axis_size("tp")
    n_ep = lax.axis_size("ep")
    tp_index = lax.axis_index("tp")
    local_rows = tokens_b.shape[0]
    block_rows = local_rows // n_tp
    picks = block_rows * TOPK
    local_experts = gate_weight.shape[0]
    assigned = routes.reshape(n_tp, picks)
    onehot = (assigned[:, :, None] == jnp.arange(EXPERTS, dtype=jnp.int32)[None, None, :]).astype(
        jnp.int32
    )
    slot_rank = jnp.sum((jnp.cumsum(onehot, axis=1) - onehot) * onehot, axis=-1)
    target = assigned * CAP + slot_rank
    target_hot = (
        target[:, :, None] == jnp.arange(EXPERTS * CAP, dtype=jnp.int32)[None, None, :]
    ).astype(jnp.float32)
    token_hot = (
        jnp.arange(picks, dtype=jnp.int32)[:, None] // TOPK
        == jnp.arange(block_rows, dtype=jnp.int32)[None, :]
    ).astype(jnp.float32)
    field = tokens_b.astype(jnp.float32)
    normed = (
        field * lax.rsqrt(jnp.mean(field * field, axis=-1, keepdims=True) + EPS) * norm_gain
    ).astype(jnp.bfloat16)
    dispatch_mat = jnp.einsum(
        "baj,at->bjt", target_hot, token_hot, precision=lax.Precision.HIGHEST
    ).astype(jnp.bfloat16)
    outgoing = jnp.einsum(
        "bjt,btd->bjd",
        dispatch_mat,
        normed.reshape(n_tp, block_rows, D),
        preferred_element_type=jnp.float32,
    )
    outgoing = outgoing.astype(jnp.bfloat16).reshape(n_tp, EXPERTS, CAP, D)
    arrived = lax.all_to_all(outgoing, "ep", split_axis=1, concat_axis=2, tiled=True)
    flat_rows = arrived.reshape(-1, D)
    share_rows = flat_rows.shape[0] // n_tp
    expert_slab_rows = flat_rows.reshape(
        share_rows * lax.axis_size("tp") // share_rows, local_experts, n_ep * CAP, D
    )
    gate_act = jnp.einsum(
        "blmd,ldf->blmf", expert_slab_rows, gate_weight, preferred_element_type=jnp.float32
    )
    up_act = jnp.einsum(
        "blmd,ldf->blmf", expert_slab_rows, up_weight, preferred_element_type=jnp.float32
    )
    hidden = (jax.nn.silu(gate_act) * up_act).astype(jnp.bfloat16)
    result = jnp.einsum("blmf,lfd->blmd", hidden, down_weight, preferred_element_type=jnp.float32)
    summed = lax.psum_scatter(
        result.reshape(-1, D).astype(jnp.bfloat16), "tp", scatter_dimension=0, tiled=True
    )
    returned = lax.all_to_all(
        summed.reshape(local_experts, n_ep, CAP, D), "ep", split_axis=1, concat_axis=0, tiled=True
    )
    returned = returned.reshape(EXPERTS * CAP, D)
    own_target = lax.dynamic_index_in_dim(target_hot, tp_index, 0, keepdims=False)
    shares = (route_weight / jnp.sum(route_weight, axis=-1, keepdims=True)).reshape(n_tp, picks)
    own_shares = lax.dynamic_index_in_dim(shares, tp_index, 0, keepdims=False)
    combine = jnp.einsum(
        "at,aj->tj", token_hot, own_target * own_shares[:, None], precision=lax.Precision.HIGHEST
    )
    return jnp.dot(combine, returned.astype(jnp.float32), precision=lax.Precision.HIGHEST).astype(
        jnp.bfloat16
    )


def on_device(
    queries,
    keys,
    values,
    query_gain,
    key_gain,
    out_weight,
    tokens_b,
    norm_gain,
    routes,
    route_weight,
    gate_weight,
    up_weight,
    down_weight,
):
    mixed_out = token_mixer(queries, keys, values, query_gain, key_gain, out_weight)
    expert_out = expert_half(
        tokens_b, norm_gain, routes, route_weight, gate_weight, up_weight, down_weight
    )
    return (mixed_out, expert_out)


def solution(mesh):
    placed = (
        P("ep", "tp"),
        P("ep", None),
        P("ep", None),
        P(),
        P(),
        P("tp", None),
        P("ep", None),
        P(),
        P("ep", None),
        P("ep", None),
        P("ep", None, "tp"),
        P("ep", None, "tp"),
        P("ep", "tp", None),
    )
    return jax.shard_map(
        on_device,
        mesh=mesh,
        in_specs=placed,
        out_specs=(P(("ep", "tp"), None), P(("ep", "tp"), None)),
        check_vma=False,
    )
```

profile of v0, /device:TPU:0, one launch (start us, length us, event | category | flops | bytes accessed | tf_op | source)
XLA Modules:
  0.0 199.7 jit_solution(16089087401707294677)
XLA Ops:
  7.2 0.0 copy-start
  7.2 1.9 fusion.24
  9.1 0.8 copy.47
  9.9 0.1 reshape.432
  10.0 0.1 copy.48
  10.1 1.9 select_reduce_fusion
  12.1 0.1 copy.49
  12.1 0.3 convolution_convert_fusion.2
  12.5 1.8 fusion.26
  14.3 1.3 convert_bitcast_fusion.1
  15.6 2.3 %copy.51 = bf16[8,16,8,2048]{3,2,0,1:T(8,128)(2,1)} copy(bf16[8,16,8,2048]{3,2,1,0:T(8,128)(2,1)S(1)} %convert_bitcast_fusion.1) | data formatting | bytes 8388608 | tf_op jit(solution)/shard_map/reshape | solution.py:126
  17.9 5.3 %all-to-all-start = ((bf16[8,16,8,2048]{3,2,0,1:T(8,128)(2,1)}), bf16[8,16,8,2048]{3,2,0,1:T(8,128)(2,1)}, u32[]{:S(2)}, u32[]{:S(2)}) async-start(bf16[8,16,8,2048]{3,2,0,1:T(8,128)(2,1)} %copy.51), calls=%async_computation.1 | async-start | bytes 8388608 | tf_op jit(solution)/shard_map/all_to_all | solution.py:127
  23.2 0.1 mul.305
  23.3 0.0 copy-done.1
  23.3 0.2 copy.44
  23.5 0.1 broadcast_multiply_fusion.1
  23.6 0.7 fusion.48
  24.3 0.1 bitcast_reduce_fusion
  24.4 0.1 multiply_multiply_fusion
  24.5 0.1 subtract_convert_fusion
  24.7 47.1 %all-to-all-done = bf16[8,16,8,2048]{3,2,0,1:T(8,128)(2,1)} async-done(((bf16[8,16,8,2048]{3,2,0,1:T(8,128)(2,1)}), bf16[8,16,8,2048]{3,2,0,1:T(8,128)(2,1)}, u32[]{:S(2)}, u32[]{:S(2)}) %all-to-all-start) | async-done | bytes 4194336 | tf_op jit(solution)/shard_map/all_to_all | solution.py:127
  71.8 8.4 %fusion.16 = f32[4,8,32,512]{3,2,1,0:T(8,128)} fusion(bf16[4,2048,512]{2,1,0:T(8,128)(2,1)} %param.25, bf16[8,4,4,8,2048]{4,3,0,2,1:T(8,128)(2,1)} %bitcast.11), kind=kOutput, calls=%fused_computation.22 | convolution fusion | flops 2147483648 | bytes 14680064 | tf_op jit(solution)/shard_map/blmd,ldf->blmf/dot_general | solution.py:133
  80.2 14.2 %convert_bitcast_fusion = bf16[8,4,32,2048]{3,2,0,1:T(8,128)(2,1)} fusion(bf16[4,512,2048]{2,1,0:T(8,128)(2,1)} %param.27, f32[4,8,32,512]{3,2,1,0:T(8,128)} %fusion.16, bf16[4,2048,512]{2,1,0:T(8,128)(2,1)} %param.26, bf16[8,4,4,8,2048]{4,3,0,2,1:T(8,128)(2,1)} %bitcast.11), kind=kOutput, calls=%fused_computation.26 | convolution fusion | flops 4300210176 | bytes 27262976 | tf_op jit(solution)/shard_map/blmf,lfd->blmd/dot_general | solution.py:140
  94.4 4.7 %copy.53 = bf16[8,4,32,2048]{3,2,1,0:T(8,128)(2,1)} copy(bf16[8,4,32,2048]{3,2,0,1:T(8,128)(2,1)} %convert_bitcast_fusion) | data formatting | bytes 8388608 | tf_op jit(solution)/shard_map/convert_element_type | solution.py:142
  99.1 0.0 reduce-scatter.5.cloned.1.call-update
  99.1 0.2 reduce-scatter.3.cloned.1.call-start
  99.3 0.9 constant_dynamic-slice_fusion.2
  100.3 0.1 copy.59
  100.5 2.9 %copy.45 = bf16[768,2,2,2,32]{4,3,2,1,0:T(2,128)(2,1)} copy(bf16[768,2,2,2,32]{0,4,3,2,1:T(8,128)(2,1)S(1)} %pad_maximum_fusion) | data formatting | bytes 786432 | tf_op jit(solution)/shard_map/stack | solution.py:32
  103.4 3.7 %convert_element_type.88 = bf16[1536,128]{1,0:T(8,128)(2,1)S(1)} reshape(bf16[768,2,2,2,32]{4,3,2,1,0:T(2,128)(2,1)} %copy.45) | data formatting | bytes 786432 | tf_op jit(solution)/shard_map/convert_element_type | solution.py:42
  107.1 0.9 constant_dynamic-slice_fusion.1
  108.0 0.1 fusion.44
  108.1 0.1 fusion.45
  108.2 0.7 subtract_convert_fusion.1
  109.0 12.7 %all_gather.6 = bf16[3072,128]{0,1:T(8,128)(2,1)S(1)} all-gather(bf16[768,128]{0,1:T(8,128)(2,1)S(1)} %bitcast.98), channel_id=1, replica_groups=mesh['ep'=4,'tp'=8] {'ep'}, dimensions={0}, use_global_device_ids=true | all-gather | bytes 983040 | tf_op jit(solution)/shard_map/all_gather | solution.py:61
  121.7 11.2 %all_gather.7 = bf16[3072,128]{1,0:T(8,128)(2,1)} all-gather(bf16[768,128]{1,0:T(8,128)(2,1)S(1)} %constant_dynamic-slice_fusion.1), channel_id=1, replica_groups=mesh['ep'=4,'tp'=8] {'ep'}, dimensions={0}, use_global_device_ids=true | all-gather | bytes 983040 | tf_op jit(solution)/shard_map/all_gather | solution.py:62
  132.9 15.4 %while.18 = (s32[]{:T(128)}, f32[1536]{0:T(1024)S(1)}, f32[1536]{0:T(1024)S(1)}, f32[1536,128]{1,0:T(8,128)S(1)}, bf16[3072,128]{0,1:T(8,128)(2,1)S(1)}, /*index...) while((s32[]{:T(128)}, f32[1536]{0:T(1024)S(1)}, ...), condition=%wide.region_5.6_spmd.clone, body=%wide.region_2.5_spmd.clone.sunk | while | flops 614014464 | bytes 16613559 | solution.py:82
  132.9 0.8 multiply_reduce_fusion.2
  133.8 0.8 fusion.86
  134.6 2.1 %convolution_add_fusion.2 = f32[1536,128]{1,0:T(8,128)S(1)} fusion(f32[768,1536]{1,0:T(8,128)S(1)} %get-tuple-element.254, f32[1536]{0:T(1024)S(1)} %select_maximum_fusion.2, f32[1536,128]{1,0:T(8,128)S(1)} %get-tuple-element.271, f32[1536]{0:T(1024)S(1)} %get-tuple-element.256, pred[]{:T(512)S(6)} %compare.22, ...), kind=kOutput, calls=%fused_computation.4.clone.1 | convolution fusion | flops 306118656 | bytes 6500357 | tf_op jit(solution)/shard_map/while/body/eval_jaxpr/dot_general | solution.py:77
  136.8 0.8 multiply_reduce_fusion.2
  137.6 0.8 fusion.86
  138.4 2.1 %convolution_add_fusion.2 = f32[1536,128]{1,0:T(8,128)S(1)} fusion(f32[768,1536]{1,0:T(8,128)S(1)} %get-tuple-element.254, f32[1536]{0:T(1024)S(1)} %select_maximum_fusion.2, f32[1536,128]{1,0:T(8,128)S(1)} %get-tuple-element.271, f32[1536]{0:T(1024)S(1)} %get-tuple-element.256, pred[]{:T(512)S(6)} %compare.22, ...), kind=kOutput, calls=%fused_computation.4.clone.1 | convolution fusion | flops 306118656 | bytes 6500357 | tf_op jit(solution)/shard_map/while/body/eval_jaxpr/dot_general | solution.py:77
  140.6 0.8 multiply_reduce_fusion.2
  141.5 0.8 fusion.86
  142.3 2.2 %convolution_add_fusion.2 = f32[1536,128]{1,0:T(8,128)S(1)} fusion(f32[768,1536]{1,0:T(8,128)S(1)} %get-tuple-element.254, f32[1536]{0:T(1024)S(1)} %select_maximum_fusion.2, f32[1536,128]{1,0:T(8,128)S(1)} %get-tuple-element.271, f32[1536]{0:T(1024)S(1)} %get-tuple-element.256, pred[]{:T(512)S(6)} %compare.22, ...), kind=kOutput, calls=%fused_computation.4.clone.1 | convolution fusion | flops 306118656 | bytes 6500357 | tf_op jit(solution)/shard_map/while/body/eval_jaxpr/dot_general | solution.py:77
  144.5 0.8 multiply_reduce_fusion.2
  145.3 0.8 fusion.86
  146.1 2.2 %convolution_add_fusion.2 = f32[1536,128]{1,0:T(8,128)S(1)} fusion(f32[768,1536]{1,0:T(8,128)S(1)} %get-tuple-element.254, f32[1536]{0:T(1024)S(1)} %select_maximum_fusion.2, f32[1536,128]{1,0:T(8,128)S(1)} %get-tuple-element.271, f32[1536]{0:T(1024)S(1)} %get-tuple-element.256, pred[]{:T(512)S(6)} %compare.22, ...), kind=kOutput, calls=%fused_computation.4.clone.1 | convolution fusion | flops 306118656 | bytes 6500357 | tf_op jit(solution)/shard_map/while/body/eval_jaxpr/dot_general | solution.py:77
  148.3 0.3 divide_convert_fusion
  148.6 0.1 reshape.431
  148.7 0.0 copy-start.2
  148.8 2.7 %convolution_convert_fusion = bf16[768,2048]{1,0:T(8,128)(2,1)} fusion(bf16[768,256]{1,0:T(8,128)(2,1)S(1)} %reshape.431, bf16[256,2048]{1,0:T(8,128)(2,1)S(1)} %copy-done), kind=kOutput, calls=%fused_computation.32 | convolution fusion | flops 806879232 | bytes 4587520 | tf_op jit(solution)/shard_map/dot_general | solution.py:85
  151.4 0.0 reduce-scatter.3.cloned.1.call-update
  151.5 0.2 iota_compare_fusion
  151.7 0.0 reduce-scatter.5.cloned.1.call-done
  151.7 1.9 copy.54
  153.6 3.5 %all-to-all-start.1 = ((bf16[4,4,8,2048]{3,2,0,1:T(8,128)(2,1)}), bf16[4,4,8,2048]{3,2,0,1:T(8,128)(2,1)S(1)}, u32[]{:S(2)}, u32[]{:S(2)}) async-start(bf16[4,4,8,2048]{3,2,0,1:T(8,128)(2,1)} %copy.54), calls=%async_computation.3 | async-start | bytes 1048576 | tf_op jit(solution)/shard_map/all_to_all | solution.py:144
  157.1 0.1 copy.50
  157.2 0.1 reshape.433
  157.4 0.2 fusion.51
  157.6 6.0 %all-to-all-done.1 = bf16[4,4,8,2048]{3,2,0,1:T(8,128)(2,1)S(1)} async-done(((bf16[4,4,8,2048]{3,2,0,1:T(8,128)(2,1)}), bf16[4,4,8,2048]{3,2,0,1:T(8,128)(2,1)S(1)}, u32[]{:S(2)}, u32[]{:S(2)}) %all-to-all-start.1) | async-done | bytes 524320 | tf_op jit(solution)/shard_map/all_to_all | solution.py:144
  163.6 1.0 convolution_convert_fusion.1
  164.6 28.2 %reduce-scatter.3.cloned.1.call-done = bf16[96,2048]{1,0:T(8,128)(2,1)} async-done(((bf16[768,2048]{1,0:T(8,128)(2,1)}), bf16[96,2048]{1,0:T(8,128)(2,1)}) %reduce-scatter.3.cloned.1.call-update) | async-done | bytes 393232 | tf_op jit(solution)/shard_map/reduce_scatter | solution.py:84
  (35 shorter events, 0.3 us)
Async XLA Ops:
  7.2 141.6 %copy-start = (bf16[256,2048]{1,0:T(8,128)(2,1)S(1)}, bf16[256,2048]{1,0:T(8,128)(2,1)}, u32[]{:S(2)}) copy-start(bf16[256,2048]{1,0:T(8,128)(2,1)} %param.20) | copy-start | bytes 3145732
  17.9 5.3 %copy-start.3 = (f32[128]{0:T(128)S(1)}, f32[128]{0:T(128)}, u32[]{:S(2)}) copy-start(f32[128]{0:T(128)} %param.18) | copy-start | bytes 1540
  17.9 5.4 %copy-start.1 = (bf16[768,256]{1,0:T(8,128)(2,1)S(1)}, bf16[768,256]{1,0:T(8,128)(2,1)}, u32[]{:S(2)}) copy-start(bf16[768,256]{1,0:T(8,128)(2,1)} %param.15) | copy-start | bytes 1179652
  17.9 53.9 %all-to-all-start = ((bf16[8,16,8,2048]{3,2,0,1:T(8,128)(2,1)}), bf16[8,16,8,2048]{3,2,0,1:T(8,128)(2,1)}, u32[]{:S(2)}, u32[]{:S(2)}) async-start(bf16[8,16,8,2048]{3,2,0,1:T(8,128)(2,1)} %copy.51), calls=%async_computation.1 | async-start | bytes 8388608 | tf_op jit(solution)/shard_map/all_to_all | solution.py:127
  23.2 128.5 %reduce-scatter.5.cloned.1.call-start = ((), (), s32[]{:S(2)}) async-start(), calls=%async_computation.5 | async-start | bytes 4718592 | tf_op jit(solution)/shard_map/reduce_scatter | solution.py:141
  99.1 9.0 %copy-start.4 = (f32[128]{0:T(128)S(1)}, f32[128]{0:T(128)}, u32[]{:S(2)}) copy-start(f32[128]{0:T(128)} %param.19) | copy-start | bytes 1540
  99.1 93.7 %reduce-scatter.3.cloned.1.call-start = ((), (), s32[]{:S(2)}) async-start(), calls=%async_computation.4 | async-start | bytes 3538944 | tf_op jit(solution)/shard_map/reduce_scatter | solution.py:84
  148.7 2.7 %copy-start.2 = (f32[384,2]{0,1:T(2,128)S(1)}, f32[384,2]{0,1:T(2,128)}, u32[]{:S(2)}) copy-start(f32[384,2]{0,1:T(2,128)} %param.24) | copy-start | bytes 9220
  153.6 10.0 %all-to-all-start.1 = ((bf16[4,4,8,2048]{3,2,0,1:T(8,128)(2,1)}), bf16[4,4,8,2048]{3,2,0,1:T(8,128)(2,1)S(1)}, u32[]{:S(2)}, u32[]{:S(2)}) async-start(bf16[4,4,8,2048]{3,2,0,1:T(8,128)(2,1)} %copy.54), calls=%async_computation.3 | async-start | bytes 1048576 | tf_op jit(solution)/shard_map/all_to_all | solution.py:144
Sparse Core Ops, SparseCore 0:
  99.2 50.3 reduce-scatter.4
  152.6 40.2 reduce-scatter.2
where the time goes:
time: 200 us
  waiting for transfers between devices  81.4 us (41%)
  matrix products  40 us (20%)
  blocking collectives  23.9 us (12%)
  local copies, waits for them, and re-layouts  19.3 us (10%)
  between operations  14.3 us (7%)
  other arithmetic  11.5 us (6%)
  starting transfers between devices  9.02 us (5%)
    all_to_all x1, waiting for transfers between devices, expert_half(): lax.all_to_all(outgoing, 'ep', split_axis=1, concat_axis=2, tiled=True)  47.1 us
    reduce_scatter x1, waiting for transfers between devices, token_mixer(): lax.psum_scatter(jnp.dot(attended, out_weight, preferred_element_type=jnp...  28.2 us
    dot_general x1, matrix products, expert_half(): jnp.einsum('blmf,lfd->blmd', hidden, down_weight, preferred_element_type=...  14.2 us
    all_gather x1, blocking collectives, token_mixer(): key_piece = lax.all_gather(own_keys, 'ep', axis=0, tiled=True)  12.7 us
    all_gather x1, blocking collectives, token_mixer(): value_piece = lax.all_gather(own_values, 'ep', axis=0, tiled=True)  11.2 us
    dot_general x4, matrix products, one_block(): jnp.dot(weights.astype(jnp.bfloat16), value_blk, preferred_element_type=j...  8.6 us
    dot_general x1, matrix products, expert_half(): jnp.einsum('blmd,ldf->blmf', expert_slab_rows, gate_weight, preferred_ele...  8.38 us
    all_to_all x1, waiting for transfers between devices, expert_half(): lax.all_to_all(summed.reshape(local_experts, n_ep, CAP, D), 'ep', split_a...  6.01 us
  transfers between devices with their start and end apart: 4, of which 3 were waited for; matrix products, arithmetic and copies ran while one was open for 16% of the time, Pallas kernels for 0%

commit v1 on v0

v1 whole, which is shorter than its diff:
```python
import functools

import jax
import jax.numpy as jnp
from jax import lax
from jax.experimental import pallas as pl
from jax.experimental.pallas import tpu as pltpu
from jax.sharding import PartitionSpec as P

HD = 128
HQ = 16
KVH = 4
EXPERTS = 16
TOPK = 2
GRID_W = 64
CAP = 8
EPS = 1e-06
THETA = 10000.0
LOG2E = 1.4426950408889634
MESH = pl.DeviceIdType.MESH
BF = jnp.bfloat16
F32 = jnp.float32


def remote(src, dst, send, recv, device):
    return pltpu.make_async_remote_copy(
        src_ref=src,
        dst_ref=dst,
        send_sem=send,
        recv_sem=recv,
        device_id=device,
        device_id_type=MESH,
    )


def turned(x, gain, cosine, sine):
    x = x.astype(F32)
    x = x * lax.rsqrt(jnp.mean(x * x, axis=-1, keepdims=True) + EPS) * gain
    lane = lax.broadcasted_iota(jnp.int32, x.shape, 1)
    partner = jnp.where(lane % 64 < 32, pltpu.roll(x, HD - 32, 1), pltpu.roll(x, 32, 1))
    return (x * cosine + partner * sine).astype(BF)


def kernel(
    n_ep,
    n_tp,
    tq,
    q_ref,
    k_ref,
    v_ref,
    cos_ref,
    sin_ref,
    qg_ref,
    kg_ref,
    wo_ref,
    tok_ref,
    ng_ref,
    route_ref,
    share_ref,
    wg_hbm,
    wu_hbm,
    wd_hbm,
    mixed_ref,
    expert_ref,
    wg,
    wu,
    wd,
    kv,
    qn,
    att,
    apart,
    asib,
    azr,
    outb,
    arr,
    part,
    sib,
    ret,
    zs,
    zr,
    w_sem,
    kv_s,
    kv_r,
    kvf_s,
    kvf_r,
    d_s,
    d_r,
    df_s,
    df_r,
    do_s,
    do_r,
    a_s,
    a_r,
    az_s,
    az_r,
    p_s,
    p_r,
    r_s,
    r_r,
    z_s,
    z_r,
):
    ep = lax.axis_index("ep")
    tp = lax.axis_index("tp")
    core = lax.rem(tp, 2)
    z = tp // 2
    n_z = n_tp // 2
    other = 1 - core
    sibling = (ep, z * 2 + other)
    ep_peers = [lax.rem(ep + k, n_ep) for k in range(1, n_ep)]
    z_peers = [lax.rem(z + k, n_z) for k in range(1, n_z)]
    n_rows = k_ref.shape[0]
    heads = q_ref.shape[1] // HD
    depth = tok_ref.shape[1]
    n_local = wg.shape[0]
    slots = n_z * CAP
    block = tok_ref.shape[0] // n_tp
    out_rows = mixed_ref.shape[0]

    weights = []
    for i in range(n_local):
        for j, (src, dst) in enumerate(((wg_hbm, wg), (wu_hbm, wu), (wd_hbm, wd))):
            copy = pltpu.make_async_copy(src.at[i], dst.at[i], w_sem.at[j, i])
            copy.start()
            weights.append(copy)

    barrier = pltpu.get_barrier_semaphore()
    for device in [sibling] + [(p, tp) for p in ep_peers] + [(ep, w * 2 + core) for w in z_peers]:
        pl.semaphore_signal(barrier, inc=1, device_id=device, device_id_type=MESH)

    cosine, sine = cos_ref[...], sin_ref[...]
    kv[0, ep] = turned(k_ref[...], kg_ref[...], cosine, sine)
    kv[1, ep] = v_ref[...]
    pl.semaphore_wait(barrier, n_ep + n_z - 1)
    sends = []
    for p in ep_peers:
        copy = remote(kv.at[core, ep], kv.at[core, ep], kv_s.at[p], kv_r.at[ep], (p, tp))
        copy.start()
        sends.append(copy)

    half = n_z * block
    route = route_ref[...]
    e_iota = lax.broadcasted_iota(jnp.int32, (EXPERTS, half), 0)
    hot0 = (e_iota == route[0:1]).astype(F32)
    hot1 = (e_iota == route[1:2]).astype(F32)
    before = lax.broadcasted_iota(jnp.int32, (half, half), 0)
    after = lax.broadcasted_iota(jnp.int32, (half, half), 1)
    earlier = ((before < after) & (before // block == after // block)).astype(F32)
    count = jnp.dot(
        (hot0 + hot1).astype(BF), earlier.astype(BF), preferred_element_type=F32
    )
    rank0 = jnp.sum(hot0 * count, axis=0, keepdims=True).astype(jnp.int32)
    rank1 = jnp.sum(hot1 * count, axis=0, keepdims=True).astype(jnp.int32)
    base = lax.broadcasted_iota(jnp.int32, (1, half), 1) // block * CAP
    slot0 = route[0:1] * slots + base + rank0
    slot1 = route[1:2] * slots + base + rank1
    j_iota = lax.broadcasted_iota(jnp.int32, (EXPERTS * slots, half), 0)
    is0 = j_iota == slot0
    is1 = j_iota == slot1
    mat = (is0 | is1).astype(F32).astype(BF)
    field = jnp.concatenate(
        [
            tok_ref[pl.ds(pl.multiple_of((2 * w + core) * block, 16), block), :]
            for w in range(n_z)
        ],
        axis=0,
    ).astype(F32)
    normed = (
        field * lax.rsqrt(jnp.mean(field * field, axis=-1, keepdims=True) + EPS) * ng_ref[...]
    ).astype(BF)
    outb[...] = (
        jnp.dot(mat, normed, preferred_element_type=F32)
        .astype(BF)
        .reshape(n_ep, n_local, slots, depth)
    )
    for p in ep_peers:
        copy = remote(outb.at[p], arr.at[:, core, ep], d_s.at[p], d_r.at[ep], (p, tp))
        copy.start()
        sends.append(copy)
    arr[:, core, ep] = outb[ep]
    copy = remote(outb.at[ep], arr.at[:, core, ep], do_s, do_r, sibling)
    copy.start()
    sends.append(copy)

    for g in range(heads):
        qn[pl.ds(g * n_rows, n_rows), :] = turned(
            q_ref[:, g * HD : (g + 1) * HD], qg_ref[...], cosine, sine
        )

    for p in ep_peers:
        remote(kv.at[core, p], kv.at[core, p], kv_s.at[p], kv_r.at[p], (p, tp)).wait_recv()
        copy = remote(kv.at[core, p], kv.at[core, p], kvf_s.at[p], kvf_r.at[p], sibling)
        copy.start()
        sends.append(copy)
    for p in ep_peers:
        remote(kv.at[other, p], kv.at[other, p], kvf_s.at[p], kvf_r.at[p], sibling).wait_recv()

    factor = HD ** (-0.5) * LOG2E
    length = n_ep * n_rows

    def attend(i, carry):
        at = pl.multiple_of(i * tq, tq)
        scores = lax.dot_general(
            qn[pl.ds(at, tq), :],
            kv[0].reshape(length, HD),
            (((1,), (1,)), ((), ())),
            preferred_element_type=F32,
        )
        top = jnp.max(scores, axis=1, keepdims=True)
        weight = jnp.exp2((scores - top) * factor)
        total = jnp.sum(weight, axis=1, keepdims=True)
        merged = jnp.dot(
            weight.astype(BF), kv[1].reshape(length, HD), preferred_element_type=F32
        )
        att[pl.ds(at, tq), :] = (merged / total).astype(BF)
        return carry

    lax.fori_loop(0, heads * n_rows // tq, attend, 0)

    def projected(t):
        total = None
        for g in range(heads):
            piece = jnp.dot(
                att[pl.ds(pl.multiple_of(g * n_rows + t * out_rows, 16), out_rows), :],
                wo_ref[pl.ds(g * HD, HD), :],
                preferred_element_type=F32,
            )
            total = piece if total is None else total + piece
        return total

    for w in range(n_z):
        apart[w] = projected(2 * w + other).astype(BF)
        copy = remote(apart.at[w], asib.at[w], a_s.at[w], a_r.at[w], sibling)
        copy.start()
        sends.append(copy)
    for w in z_peers:
        own = projected(2 * w + core)
        remote(apart.at[w], asib.at[w], a_s.at[w], a_r.at[w], sibling).wait_recv()
        asib[w] = (own + asib[w].astype(F32)).astype(BF)
        copy = remote(
            asib.at[w], azr.at[z], az_s.at[w], az_r.at[z], (ep, w * 2 + core)
        )
        copy.start()
        sends.append(copy)
    remote(apart.at[z], asib.at[z], a_s.at[z], a_r.at[z], sibling).wait_recv()
    asib[z] = (projected(2 * z + core) + asib[z].astype(F32)).astype(BF)

    for p in ep_peers:
        remote(outb.at[p], arr.at[:, core, p], d_s.at[p], d_r.at[p], (p, tp)).wait_recv()
        copy = remote(arr.at[:, core, p], arr.at[:, core, p], df_s.at[p], df_r.at[p], sibling)
        copy.start()
        sends.append(copy)
    remote(outb.at[ep], arr.at[:, other, ep], do_s, do_r, sibling).wait_recv()
    for p in ep_peers:
        remote(
            arr.at[:, other, p], arr.at[:, other, p], df_s.at[p], df_r.at[p], sibling
        ).wait_recv()

    def give_back(i):
        remote(part.at[i, other], sib.at[i], p_s.at[i], p_r.at[i], sibling).wait_recv()
        sib[i] = (part[i, core].astype(F32) + sib[i].astype(F32)).astype(BF)
        for p in ep_peers:
            copy = remote(sib.at[i, p], ret.at[ep, i], r_s.at[i, p], r_r.at[i, ep], (p, tp))
            copy.start()
            sends.append(copy)
        ret[ep, i] = sib[i, ep]

    for i in range(n_local):
        for copy in weights[3 * i : 3 * i + 3]:
            copy.wait()
        x = arr[i].reshape(2 * n_ep * slots, depth)
        gate = jnp.dot(x, wg[i], preferred_element_type=F32)
        up = jnp.dot(x, wu[i], preferred_element_type=F32)
        hidden = (gate / (1.0 + jnp.exp(-gate)) * up).astype(BF)
        part[i] = (
            jnp.dot(hidden, wd[i], preferred_element_type=F32)
            .astype(BF)
            .reshape(2, n_ep, slots, depth)
        )
        copy = remote(part.at[i, other], sib.at[i], p_s.at[i], p_r.at[i], sibling)
        copy.start()
        sends.append(copy)
        if i > 0:
            give_back(i - 1)
    give_back(n_local - 1)

    share = share_ref[...]
    share = share / jnp.sum(share, axis=0, keepdims=True)
    comb = jnp.where(is0, share[0:1], 0.0) + jnp.where(is1, share[1:2], 0.0)
    high = comb.astype(BF)
    low = (comb - high.astype(F32)).astype(BF)
    both = jnp.concatenate([high, low], axis=1)
    for p in ep_peers:
        for i in range(n_local):
            remote(
                sib.at[i, p], ret.at[p, i], r_s.at[i, p], r_r.at[i, p], (p, tp)
            ).wait_recv()
    rows = lax.dot_general(
        both,
        ret[...].reshape(EXPERTS * slots, depth),
        (((0,), (0,)), ((), ())),
        preferred_element_type=F32,
    )
    rows = rows[:half] + rows[half:]
    zs[...] = rows.astype(BF).reshape(n_z, block, depth)
    for w in z_peers:
        copy = remote(zs.at[w], zr.at[z], z_s.at[w], z_r.at[z], (ep, w * 2 + core))
        copy.start()
        sends.append(copy)

    total = asib[z].astype(F32)
    for w in z_peers:
        remote(asib.at[w], azr.at[w], az_s.at[w], az_r.at[w], (ep, w * 2 + core)).wait_recv()
        total = total + azr[w].astype(F32)
    mixed_ref[...] = total.astype(BF)
    total = zs[z].astype(F32)
    for w in z_peers:
        remote(zs.at[w], zr.at[w], z_s.at[w], z_r.at[w], (ep, w * 2 + core)).wait_recv()
        total = total + zr[w].astype(F32)
    expert_ref[...] = total.astype(BF)
    for copy in sends:
        copy.wait_send()


def on_device(
    queries,
    keys,
    values,
    query_gain,
    key_gain,
    out_weight,
    tokens_b,
    norm_gain,
    routes,
    route_weight,
    gate_weight,
    up_weight,
    down_weight,
):
    n_ep, n_tp = lax.axis_size("ep"), lax.axis_size("tp")
    ep, tp = lax.axis_index("ep"), lax.axis_index("tp")
    n_z = n_tp // 2
    n_rows = queries.shape[0]
    heads = queries.shape[1] // HD
    depth = tokens_b.shape[1]
    local_rows = tokens_b.shape[0]
    block = local_rows // n_tp
    n_local, _, ff = gate_weight.shape
    slots = n_z * CAP
    length = n_rows * n_ep
    tq = n_rows
    while tq * length > 256 * 3072:
        tq //= 2

    positions = ep * n_rows + jnp.arange(n_rows, dtype=jnp.int32)
    lane = jnp.arange(HD, dtype=jnp.int32)
    n_freq = HD // 4
    inverse = THETA ** (-(lane % n_freq).astype(F32) / n_freq)
    along = jnp.where(lane[None] < HD // 2, positions[:, None] // GRID_W, positions[:, None] % GRID_W)
    angle = along.astype(F32) * inverse
    cosine = jnp.cos(angle)
    sine = jnp.sin(angle) * jnp.where(lane % (2 * n_freq) < n_freq, -1.0, 1.0)

    kv_index = tp * heads // (HQ // KVH)
    own_keys = lax.dynamic_slice_in_dim(keys, kv_index * HD, HD, 1)
    own_values = lax.dynamic_slice_in_dim(values, kv_index * HD, HD, 1)

    def mine(table):
        split = table.reshape(n_z, 2, block, TOPK)
        own = lax.dynamic_index_in_dim(split, lax.rem(tp, 2), 1, keepdims=False)
        return own.reshape(n_z * block, TOPK).T

    vmem = pl.BlockSpec(memory_space=pltpu.VMEM)
    hbm = pl.BlockSpec(memory_space=pl.ANY)
    dma = pltpu.SemaphoreType.DMA
    out_rows = n_rows // n_tp
    scratch = [
        pltpu.VMEM(gate_weight.shape, BF),
        pltpu.VMEM(up_weight.shape, BF),
        pltpu.VMEM(down_weight.shape, BF),
        pltpu.VMEM((2, n_ep, n_rows, HD), BF),
        pltpu.VMEM((heads * n_rows, HD), BF),
        pltpu.VMEM((heads * n_rows, HD), BF),
        pltpu.VMEM((n_z, out_rows, depth), BF),
        pltpu.VMEM((n_z, out_rows, depth), BF),
        pltpu.VMEM((n_z, out_rows, depth), BF),
        pltpu.VMEM((n_ep, n_local, slots, depth), BF),
        pltpu.VMEM((n_local, 2, n_ep, slots, depth), BF),
        pltpu.VMEM((n_local, 2, n_ep, slots, depth), BF),
        pltpu.VMEM((n_local, n_ep, slots, depth), BF),
        pltpu.VMEM((n_ep, n_local, slots, depth), BF),
        pltpu.VMEM((n_z, block, depth), BF),
        pltpu.VMEM((n_z, block, depth), BF),
        dma((3, n_local)),
        dma((n_ep,)),
        dma((n_ep,)),
        dma((n_ep,)),
        dma((n_ep,)),
        dma((n_ep,)),
        dma((n_ep,)),
        dma((n_ep,)),
        dma((n_ep,)),
        dma,
        dma,
        dma((n_z,)),
        dma((n_z,)),
        dma((n_z,)),
        dma((n_z,)),
        dma((n_local,)),
        dma((n_local,)),
        dma((n_local, n_ep)),
        dma((n_local, n_ep)),
        dma((n_z,)),
        dma((n_z,)),
    ]
    return tuple(
        pl.pallas_call(
            functools.partial(kernel, n_ep, n_tp, tq),
            out_shape=(
                jax.ShapeDtypeStruct((out_rows, out_weight.shape[1]), BF),
                jax.ShapeDtypeStruct((block, depth), BF),
            ),
            in_specs=[vmem] * 12 + [hbm] * 3,
            out_specs=(vmem, vmem),
            scratch_shapes=scratch,
            compiler_params=pltpu.CompilerParams(
                collective_id=0, has_side_effects=True, vmem_limit_bytes=67043328
            ),
        )(
            queries,
            own_keys,
            own_values,
            cosine,
            sine,
            query_gain[None],
            key_gain[None],
            out_weight,
            tokens_b,
            norm_gain[None],
            mine(routes),
            mine(route_weight),
            gate_weight,
            up_weight,
            down_weight,
        )
    )


def solution(mesh):
    placed = (
        P("ep", "tp"),
        P("ep", None),
        P("ep", None),
        P(),
        P(),
        P("tp", None),
        P("ep", None),
        P(),
        P("ep", None),
        P("ep", None),
        P("ep", None, "tp"),
        P("ep", None, "tp"),
        P("ep", "tp", None),
    )
    return jax.shard_map(
        on_device,
        mesh=mesh,
        in_specs=placed,
        out_specs=(P(("ep", "tp"), None), P(("ep", "tp"), None)),
        check_vma=False,
    )
```

time: 200 us -> 103 us (0.52)
  Pallas kernels: 0 us -> 90.3 us
  waiting for transfers between devices: 81.4 us -> 0 us
  matrix products: 40 us -> 0 us
  blocking collectives: 23.9 us -> 0 us
  between operations: 14.3 us -> 0.71 us
  local copies, waits for them, and re-layouts: 19.3 us -> 8.08 us
  starting transfers between devices: 9.02 us -> 0 us
  other arithmetic: 11.5 us -> 2.83 us
    pallas_call x0 -> x1, Pallas kernels: none -> 90.3 us  [on_device(): pl.pallas_call(functools.partial(kernel, n_ep, n_tp, tq), out_shape=(jax....]
    all_to_all x2 -> x0, waiting for transfers between devices: 53.1 us -> none  [the longest x1 47.1 us: expert_half(): lax.all_to_all(outgoing, 'ep', split_axis=1, concat_axis=2, tiled=True)]
    dot_general x15 -> x0, matrix products: 40 us -> none  [the longest x1 14.2 us: expert_half(): jnp.einsum('blmf,lfd->blmd', hidden, down_weight, preferred_element_type=...]
    reduce_scatter x2 -> x0, waiting for transfers between devices: 28.2 us -> none  [the longest x1 28.2 us: token_mixer(): lax.psum_scatter(jnp.dot(attended, out_weight, preferred_element_type=jnp...]
    all_gather x2 -> x0, blocking collectives: 23.9 us -> none  [the longest x1 12.7 us: token_mixer(): key_piece = lax.all_gather(own_keys, 'ep', axis=0, tiled=True)]
    all_to_all x2 -> x0, starting transfers between devices: 8.79 us -> none  [the longest x1 5.32 us: expert_half(): lax.all_to_all(outgoing, 'ep', split_axis=1, concat_axis=2, tiled=True)]
    convert_element_type x2 -> x0, local copies, waits for them, and re-layouts: 8.41 us -> none  [the longest x1 4.7 us: expert_half(): result.reshape(-1, D).astype(jnp.bfloat16)]
    reduce_sum x8 -> x0, other arithmetic: 5.26 us -> none  [the longest x4 3.21 us: one_block(): totals = totals * shrink + jnp.sum(weights, axis=1)]
  transfers between devices with their start and end apart: 4 -> 0, of which waited for: 3 -> 0; matrix products, arithmetic and copies ran while one was open for 16% -> 0% of each run, Pallas kernels for 0% -> 0%
where the time goes in v1:
time: 103 us; the launch traced here: 102 us
  Pallas kernels  90.3 us (88%)
  local copies, waits for them, and re-layouts  8.08 us (8%)
  other arithmetic  2.83 us (3%)
    pallas_call x1, Pallas kernels, on_device(): pl.pallas_call(functools.partial(kernel, n_ep, n_tp, tq), out_shape=(jax....  90.3 us
    unnamed x2, local copies, waits for them, and re-layouts  3.38 us
    mul x1, other arithmetic, on_device(): sine = jnp.sin(angle) * jnp.where(lane % (2 * n_freq) < n_freq, -1.0, 1.0)  2.8 us

profile of v1, /device:TPU:0, one launch (start us, length us, event | category | flops | bytes accessed | tf_op | source)
XLA Modules:
  0.0 101.9 jit_solution(17295568379987248510)
XLA Ops:
  0.7 0.8 reshape.103
  1.5 0.7 reshape.104
  2.2 0.8 reshape.105
  3.0 0.7 reshape.106
  3.6 1.8 %constant_dynamic-slice_fusion.2 = (bf16[768,128]{1,0:T(8,128)(2,1)}, bf16[768,128]{1,0:T(8,128)(2,1)}) fusion(bf16[768,512]{1,0:T(8,128)(2,1)} %param.15, s32[]{:T(128)S(6)} %select_n.67, bf16[768,512]{1,0:T(8,128)(2,1)} %param.14), kind=kLoop, calls=%fused_computation.20 | loop fusion | bytes 786436 | tf_op jit(solution)/shard_map/dynamic_slice | solution.py:366
  5.4 2.8 %sine_multiply_fusion = (f32[768,128]{1,0:T(8,128)}, f32[768,128]{1,0:T(8,128)}) fusion(f32[128]{0:T(128)S(1)} %get-tuple-element.4, f32[128]{0:T(128)S(1)} %get-tuple-element.5, s32[768]{0:T(1024)S(1)} %get-tuple-element.8, s32[768]{0:T(1024)S(1)} %get-tuple-element.9, pred[128]{0:T(512)(128)(4,1)S(1)} %iota_compare_fusion), kind=kLoop, calls=%fused_computation | loop fusion | flops 393216 | bytes 793728 | tf_op jit(solution)/shard_map/mul | solution.py:362
  8.2 90.3 %shard_map.140 = (bf16[96,2048]{1,0:T(8,128)(2,1)}, bf16[48,2048]{1,0:T(8,128)(2,1)}) custom-call(bf16[768,256]{1,0:T(8,128)(2,1)} %q_ref.1, bf16[768,128]{1,0:T(8,128)(2,1)} %get-tuple-element.7.k_ref, bf16[768,128]{1,0:T(8,128)(2,1)} %get-tuple-element.6.v_ref, f32[768,128]{1,0:T(8,128)} %get-tuple-element.3.cos_ref, f32[768,128]{1,0:T(8,128)} %get-tuple-element.2.sin_ref, ...), custom_call_target="tpu_custom_call" | custom-call | tf_op jit(solution)/shard_map/pallas_call | solution.py:417
  98.5 1.8 %copy.21 = bf16[96,2048]{1,0:T(8,128)(2,1)} copy(bf16[96,2048]{1,0:T(8,128)(2,1)} %get-tuple-element.12) | data formatting | bytes 786432
  100.3 1.6 %copy.22 = bf16[48,2048]{1,0:T(8,128)(2,1)} copy(bf16[48,2048]{1,0:T(8,128)(2,1)} %get-tuple-element.13) | data formatting | bytes 393216
  (5 shorter events, 0.0 us)
